TPU v7x, 32 devices: a whole 2x2x4 slice. The times are simulated.
32 devices in a mesh: sp: 16 (over z, y, x), tp: 2 (over core).
Axes of the slice: x: 2, y: 2, z: 4, core: 2. Of those that a mesh axis runs over, the one named last changes fastest.
Arguments:
- skip_path_inputs: bfloat16 [2048, 2048], P('sp'), may hold values from -62 to 62
- probe_vectors: bfloat16 [2048, 1024], P('sp', 'tp'), may hold values from -6 to 6
- lookup_vectors: bfloat16 [2048, 1024], P('sp', 'tp'), may hold values from -6 to 6
- payload_vectors: bfloat16 [2048, 1024], P('sp', 'tp'), may hold values from -6 to 6
- learning_strength_preacts: float32 [2, 2048, 8], P(None, 'sp', 'tp'), may hold values from -6 to 6
- forget_preacts: float32 [2, 2048, 8], P(None, 'sp', 'tp'), may hold values from -5 to 5
- forgetting_speed_exponent: float32 [2, 8], P(None, 'tp'), may hold values from -12 to -2
- extra_forgetting_spikes: float32 [2, 2048, 8], P(None, 'sp', 'tp'), may hold values from -0.7 to 0
- sample_membership: int32 [2048], P('sp'), may hold values from 0 to 3, never falling along the last dimension, each value on 1 to 1024 neighbouring positions
- channel_group_scaling: float32 [128], replicated, may hold values from 0.1 to 1.9
- blend_exit_weights: bfloat16 [1024, 2048], P('tp'), may hold values from -0.1875 to 0.1875
- dense_block_scaling: float32 [2048], replicated, may hold values from 0.1 to 1.9
- widen_projection_weights: bfloat16 [2048, 8192], P('sp', 'tp'), may hold values from -0.125 to 0.125
- shrink_projection_weights: bfloat16 [8192, 2048], P('tp', 'sp'), may hold values from -0.0625 to 0.0625
Outputs:
- result: bfloat16 [2048, 2048], P('sp', 'tp')
Inputs may be any that keep to these rules, and one draw needn't show every extreme that they name: `sample_membership`: document numbers never fall along the positions; each document holds 1 to 1024 positions.
All inputs are finite; a program needn't handle non-finite values.
Results may differ from a plain program's by a relative error of at most 0.015.
Values may be sent and summed in bfloat16 or wider, within the bound.
A program may use at most 128 MiB of HBM per device.

v0:
```python
import jax
import jax.numpy as jnp
from jax import lax
from jax.sharding import PartitionSpec as P

BLOCK = 64


HIGH = lax.Precision.HIGHEST
EPSILON = 1e-06


def entering(array, axis, combine, identity, reverse):
    length, here = (lax.axis_size(axis), lax.axis_index(axis))
    everything = jax.tree.map(
        lambda part, kind: lax.all_gather(part.astype(kind), axis),
        array,
        jax.tree.map(lambda a: jnp.bfloat16 if a.dtype == jnp.float32 else a.dtype, array),
    )
    start = jax.tree.map(
        lambda part, zero: jnp.broadcast_to(jnp.asarray(zero, part.dtype), part.shape),
        array,
        identity,
    )

    def hop(k, before):
        at = length - 1 - k if reverse else k
        reached = at > here if reverse else at < here
        new = combine(
            before, jax.tree.map(lambda part, own: part[at].astype(own.dtype), everything, array)
        )
        return jax.tree.map(lambda a, b: jnp.where(reached, a, b), new, before)

    return lax.fori_loop(0, length, hop, start)


def block_pass(
    memory,
    probe_vectors,
    lookup_vectors,
    payload_vectors,
    strengths,
    forget_multipliers,
    doc_ids,
    prior_doc,
    wanted,
):
    value_width = payload_vectors.shape[-1]
    block_len = probe_vectors.shape[1]
    running = jnp.cumsum(forget_multipliers, axis=-1)
    row_ids = lax.broadcasted_iota(jnp.int32, (block_len, block_len), 0)
    col_ids = lax.broadcasted_iota(jnp.int32, (block_len, block_len), 1)
    shared = doc_ids[:, None] == doc_ids[None, :]
    within = (row_ids >= col_ids) & shared
    before = (row_ids > col_ids) & shared
    spread = jnp.exp(jnp.where(within, running[:, :, None] - running[:, None, :], -jnp.inf))
    linked = (doc_ids == prior_doc).astype(jnp.float32)
    ending = (doc_ids == doc_ids[-1]).astype(jnp.float32)
    weighted = lookup_vectors * strengths[..., None]
    system = jnp.eye(block_len, dtype=jnp.float32) + jnp.where(
        before, jnp.einsum("hik,hjk->hij", weighted, lookup_vectors, precision=HIGH) * spread, 0.0
    )
    right_side = jnp.concatenate(
        [payload_vectors * strengths[..., None], weighted * (jnp.exp(running) * linked)[..., None]],
        axis=-1,
    )
    solved = jax.scipy.linalg.solve_triangular(system, right_side, lower=True, unit_diagonal=True)
    update = solved[..., :value_width] - jnp.einsum(
        "hck,hkw->hcw", solved[..., value_width:], memory, precision=HIGH
    )
    faded_keys = lookup_vectors * (jnp.exp(running[:, -1:] - running) * ending)[..., None]
    kept_share = jnp.exp(running[:, -1]) * linked[-1]
    renewed = memory * kept_share[:, None, None] + jnp.einsum(
        "hck,hcw->hkw", faded_keys, update, precision=HIGH
    )
    if not wanted:
        return (renewed, None)
    scores = jnp.where(
        within,
        jnp.einsum("hik,hjk->hij", probe_vectors, lookup_vectors, precision=HIGH) * spread,
        0.0,
    )
    reading = jnp.einsum(
        "hck,hkw->hcw",
        probe_vectors * (jnp.exp(running) * linked)[..., None],
        memory,
        precision=HIGH,
    )
    return (renewed, reading + jnp.einsum("hij,hjw->hiw", scores, update, precision=HIGH))


def run_blocks(
    memory,
    prior_doc,
    probe_vectors,
    lookup_vectors,
    payload_vectors,
    strengths,
    forget_multipliers,
    doc_ids,
    wanted,
):
    head_count, length, key_width = probe_vectors.shape
    block_count = length // BLOCK

    def split_blocks(tensor):
        return jnp.moveaxis(
            tensor.reshape((head_count, block_count, BLOCK) + tensor.shape[2:]), 1, 0
        )

    def advance(carried, inputs):
        held, earlier_doc = carried
        query_block, key_block, value_block, gate_block, decay_block, doc_block = inputs
        held, produced = block_pass(
            held,
            query_block,
            key_block,
            value_block,
            gate_block,
            decay_block,
            doc_block,
            earlier_doc,
            wanted,
        )
        return ((held, doc_block[-1]), produced)

    (final, _), produced = lax.scan(
        advance,
        (memory, prior_doc),
        (
            split_blocks(probe_vectors),
            split_blocks(lookup_vectors),
            split_blocks(payload_vectors),
            split_blocks(strengths),
            split_blocks(forget_multipliers),
            doc_ids.reshape(block_count, BLOCK),
        ),
    )
    if wanted:
        produced = jnp.moveaxis(produced, 0, 1).reshape(head_count, length, -1)
    return (final, produced)


def unit_rows(tensor):
    return tensor * lax.rsqrt(jnp.sum(tensor * tensor, axis=-1, keepdims=True) + EPSILON)


def heads_first(tensor, head_width):
    row_count = tensor.shape[0]
    return jnp.transpose(tensor.astype(jnp.float32).reshape(row_count, -1, head_width), (1, 0, 2))


def summarize(
    probe_vectors, lookup_vectors, payload_vectors, strengths, forget_multipliers, doc_ids
):
    head_count, length, key_width = probe_vectors.shape
    start_map = jnp.concatenate(
        [
            jnp.broadcast_to(
                jnp.eye(key_width, dtype=jnp.float32), (head_count, key_width, key_width)
            ),
            jnp.zeros((head_count, key_width, payload_vectors.shape[-1]), jnp.float32),
        ],
        axis=-1,
    )
    padded = jnp.concatenate(
        [jnp.zeros((head_count, length, key_width), jnp.float32), payload_vectors], axis=-1
    )
    final, _ = run_blocks(
        start_map,
        doc_ids[0],
        probe_vectors,
        lookup_vectors,
        padded,
        strengths,
        forget_multipliers,
        doc_ids,
        False,
    )
    as_float = doc_ids.astype(jnp.float32)
    return (final[..., :key_width], final[..., key_width:], as_float[0], as_float[-1])


def compose(earlier, later):
    early_map, early_shift, early_first, early_last = earlier
    late_map, late_shift, late_first, late_last = later
    joined = ((late_first == early_last) | (early_last < 0) | (late_first < 0)).astype(jnp.float32)
    new_map = jnp.einsum("hij,hjk->hik", late_map, early_map, precision=HIGH) * joined
    new_shift = (
        jnp.einsum("hij,hjk->hik", late_map, early_shift, precision=HIGH) * joined + late_shift
    )
    return (
        new_map,
        new_shift,
        jnp.where(early_first < 0, late_first, early_first),
        jnp.where(late_last < 0, early_last, late_last),
    )


def neutral(head_count, key_width, value_width):
    return (
        jnp.broadcast_to(jnp.eye(key_width, dtype=jnp.float32), (head_count, key_width, key_width)),
        jnp.zeros((head_count, key_width, value_width), jnp.float32),
        jnp.full((), -1.0, jnp.float32),
        jnp.full((), -1.0, jnp.float32),
    )


def shards(
    skip_path_inputs,
    probe_vectors,
    lookup_vectors,
    payload_vectors,
    learning_strength_preacts,
    forget_preacts,
    forgetting_speed_exponent,
    extra_forgetting_spikes,
    sample_membership,
    channel_group_scaling,
    blend_exit_weights,
    dense_block_scaling,
    widen_projection_weights,
    shrink_projection_weights,
):
    length = probe_vectors.shape[0]
    key_width = channel_group_scaling.shape[0]
    query_heads = unit_rows(heads_first(probe_vectors, key_width)) * key_width ** (-0.5)
    key_heads = unit_rows(heads_first(lookup_vectors, key_width))
    value_heads = heads_first(payload_vectors, key_width)
    head_count = query_heads.shape[0]
    strengths = jnp.transpose(jax.nn.sigmoid(learning_strength_preacts), (0, 2, 1))
    forget_multipliers = jnp.transpose(
        -jnp.exp(forgetting_speed_exponent)[:, None, :] * jax.nn.softplus(forget_preacts)
        + extra_forgetting_spikes,
        (0, 2, 1),
    )
    forward_parts = summarize(
        query_heads, key_heads, value_heads, strengths[0], forget_multipliers[0], sample_membership
    )
    forward_prefix = entering(
        forward_parts, "sp", compose, neutral(head_count, key_width, key_width), False
    )
    _, forward_out = run_blocks(
        forward_prefix[1],
        forward_prefix[3].astype(jnp.int32),
        query_heads,
        key_heads,
        value_heads,
        strengths[0],
        forget_multipliers[0],
        sample_membership,
        True,
    )
    flipped_queries = jnp.flip(query_heads, 1)
    flipped_keys = jnp.flip(key_heads, 1)
    flipped_values = jnp.flip(value_heads, 1)
    flipped_gates = jnp.flip(strengths[1], 1)
    flipped_decays = jnp.flip(forget_multipliers[1], 1)
    flipped_docs = jnp.flip(sample_membership, 0)
    backward_parts = summarize(
        flipped_queries, flipped_keys, flipped_values, flipped_gates, flipped_decays, flipped_docs
    )
    backward_prefix = entering(
        backward_parts, "sp", compose, neutral(head_count, key_width, key_width), True
    )
    _, backward_out = run_blocks(
        backward_prefix[1],
        backward_prefix[3].astype(jnp.int32),
        flipped_queries,
        flipped_keys,
        flipped_values,
        flipped_gates,
        flipped_decays,
        flipped_docs,
        True,
    )
    attn = forward_out + jnp.flip(backward_out, 1)
    scaled = (
        attn
        * lax.rsqrt(jnp.mean(attn * attn, axis=-1, keepdims=True) + EPSILON)
        * channel_group_scaling
    )
    mixed = (
        jnp.transpose(scaled, (1, 0, 2))
        .reshape(length, head_count * key_width)
        .astype(jnp.bfloat16)
    )
    head_terms = lax.optimization_barrier(
        jnp.dot(mixed, blend_exit_weights, preferred_element_type=jnp.float32).astype(jnp.bfloat16)
    ).astype(jnp.float32)
    model_width = skip_path_inputs.shape[1]
    col_count = model_width // lax.axis_size("tp")
    col_start = lax.axis_index("tp") * col_count
    summed = lax.psum(head_terms.astype(jnp.bfloat16), "tp").astype(jnp.float32)
    residual = skip_path_inputs.astype(jnp.float32) + summed
    normed = (
        residual
        * lax.rsqrt(jnp.mean(residual * residual, axis=1, keepdims=True) + EPSILON)
        * dense_block_scaling
    ).astype(jnp.bfloat16)
    own_residual = lax.dynamic_slice_in_dim(residual, col_start, col_count, 1)
    raised = jnp.dot(
        normed,
        lax.all_gather(widen_projection_weights, "sp", axis=0, tiled=True),
        preferred_element_type=jnp.float32,
    )
    active = jnp.square(jax.nn.relu(raised)).astype(jnp.bfloat16)
    lowered = jnp.dot(
        active,
        lax.all_gather(shrink_projection_weights, "sp", axis=1, tiled=True),
        preferred_element_type=jnp.float32,
    )
    rounded = lax.optimization_barrier(lowered.astype(jnp.bfloat16)).astype(jnp.float32)
    mixer_cols = lax.psum_scatter(
        rounded.astype(jnp.bfloat16), "tp", scatter_dimension=1, tiled=True
    ).astype(jnp.float32)
    return (own_residual + mixer_cols).astype(jnp.bfloat16)


def solution(mesh):
    placed = (
        P("sp", None),
        P("sp", "tp"),
        P("sp", "tp"),
        P("sp", "tp"),
        P(None, "sp", "tp"),
        P(None, "sp", "tp"),
        P(None, "tp"),
        P(None, "sp", "tp"),
        P("sp"),
        P(),
        P("tp", None),
        P(),
        P("sp", "tp"),
        P("tp", "sp"),
    )
    return jax.shard_map(
        shards, mesh=mesh, in_specs=placed, out_specs=P("sp", "tp"), check_vma=False
    )
```

profile of v0, /device:TPU:0, one launch (start us, length us, event | category | flops | bytes accessed | tf_op | source)
XLA Modules:
  0.0 1001.6 jit_solution(841433032563091980)
XLA Ops:
  7.5 1.3 fusion.158
  15.5 1.8 concatenate.24.clone
  17.3 59.1 %while.88 = (s32[]{:T(128)}, f32[4,128,256]{2,1,0:T(8,128)S(1)}, s32[]{:T(128)}, f32[2,4,64]{2,1,0:T(4,128)}, s32[2,64]{1,0:T(2,128)}, /*index=5*/f32[2,4,64,128...) while((s32[]{:T(128)}, f32[4,128,256]{2,1,0:T(8,128)S(1)}, ...), condition=%wide.region_12.15_spmd, body=%wide.region_10.14_spmd.sunk | while | flops 302785408 | bytes 4747572 | solution.py:127
  20.7 20.4 %custom-call.20 = f32[4,1,64,64]{2,3,1,0:T(8,128)S(1)} custom-call(f32[4,1,64,64]{3,2,1,0:T(8,128)} %fusion.286), custom_call_target="InvertDiagBlocksLowerTriangular" | custom-call | tf_op jit(solution)/shard_map/while/body/eval_jaxpr/jit(_solve_triangular)/vmap()/triangular_solve | solution.py:67
  50.2 20.4 %custom-call.20 = f32[4,1,64,64]{2,3,1,0:T(8,128)S(1)} custom-call(f32[4,1,64,64]{3,2,1,0:T(8,128)} %fusion.286), custom_call_target="InvertDiagBlocksLowerTriangular" | custom-call | tf_op jit(solution)/shard_map/while/body/eval_jaxpr/jit(_solve_triangular)/vmap()/triangular_solve | solution.py:67
  78.1 1.8 copy.86
  84.8 59.3 %while.86 = (s32[]{:T(128)}, f32[4,128,256]{2,1,0:T(8,128)S(1)}, s32[]{:T(128)}, f32[2,4,64]{2,1,0:T(4,128)}, s32[2,64]{1,0:T(2,128)}, /*index=5*/f32[2,4,64,128...) while((s32[]{:T(128)}, f32[4,128,256]{2,1,0:T(8,128)S(1)}, ...), condition=%wide.region_3.5_spmd, body=%wide.region_1.4_spmd.sunk | while | flops 302785408 | bytes 4747572 | solution.py:127
  88.2 20.4 %custom-call.18 = f32[4,1,64,64]{2,3,1,0:T(8,128)S(1)} custom-call(f32[4,1,64,64]{3,2,1,0:T(8,128)} %fusion.256), custom_call_target="InvertDiagBlocksLowerTriangular" | custom-call | tf_op jit(solution)/shard_map/while/body/eval_jaxpr/jit(_solve_triangular)/vmap()/triangular_solve | solution.py:67
  117.8 20.4 %custom-call.18 = f32[4,1,64,64]{2,3,1,0:T(8,128)S(1)} custom-call(f32[4,1,64,64]{3,2,1,0:T(8,128)} %fusion.256), custom_call_target="InvertDiagBlocksLowerTriangular" | custom-call | tf_op jit(solution)/shard_map/while/body/eval_jaxpr/jit(_solve_triangular)/vmap()/triangular_solve | solution.py:67
  149.9 1.9 reverse.4
  152.6 1.8 copy.109
  155.1 1.4 dynamic-update-slice.2
  156.5 1.5 dynamic-update-slice.3
  158.0 1.4 dynamic-update-slice
  159.4 1.3 dynamic-update-slice.1
  160.7 1.8 copy.95
  162.5 45.0 %all-reduce.7 = (bf16[16]{0:T(256)(128)(2,1)S(1)}, bf16[16]{0:T(256)(128)(2,1)S(1)}, bf16[16]{0:T(256)(128)(2,1)}, bf16[16]{0:T(256)(128)(2,1)}) all-reduce(bf16[16]{0:T(256)(128)(2,1)S(1)} %dynamic-update-slice.2, bf16[16]{0:T(256)(128)(2,1)S(1)} %dynamic-update-slice.3, ...), channel_id=1, replica_groups=mesh['sp'=16,'tp'=2] {'sp'}, use_global_device_ids=true, to_apply=%add.5 | all-reduce | flops 64 | bytes 256
  207.5 74.9 %while.91 = (s32[]{:T(128)}, f32[4,128,128]{2,1,0:T(8,128)S(1)}, f32[]{:T(128)}, s32[]{:T(128)}, bf16[16,4,128,128]{3,2,1,0:T(8,128)(2,1)}, /*index=5*/bf16[16]{...) while((s32[]{:T(128)}, f32[4,128,128]{2,1,0:T(8,128)S(1)}, ...), condition=%wide.region_14.17_spmd.clone, body=%wide.region_13.16_spmd.clone.sunk | while | flops 101056528 | bytes 1576206 | solution.py:34
  283.2 60.2 %while.89 = (s32[]{:T(128)}, f32[4,128,128]{2,1,0:T(8,128)S(1)}, s32[]{:T(128)}, f32[2,4,64,128]{3,2,0,1:T(8,128)}, f32[2,4,64]{2,1,0:T(4,128)}, /*index=5*/s32[...) while((s32[]{:T(128)}, f32[4,128,128]{2,1,0:T(8,128)S(1)}, ...), condition=%wide.region_17.20_spmd, body=%wide.region_15.19_spmd.sunk | while | flops 277521280 | bytes 7515824 | solution.py:127
  285.8 19.7 %custom-call.21 = f32[4,1,64,64]{2,3,1,0:T(8,128)S(1)} custom-call(f32[4,1,64,64]{3,2,1,0:T(8,128)S(1)} %fusion.302), custom_call_target="InvertDiagBlocksLowerTriangular" | custom-call | tf_op jit(solution)/shard_map/while/body/eval_jaxpr/jit(_solve_triangular)/vmap()/triangular_solve | solution.py:67
  315.9 19.7 %custom-call.21 = f32[4,1,64,64]{2,3,1,0:T(8,128)S(1)} custom-call(f32[4,1,64,64]{3,2,1,0:T(8,128)S(1)} %fusion.302), custom_call_target="InvertDiagBlocksLowerTriangular" | custom-call | tf_op jit(solution)/shard_map/while/body/eval_jaxpr/jit(_solve_triangular)/vmap()/triangular_solve | solution.py:67
  343.4 3.0 rev.30
  346.3 103.0 %while.90 = (s32[]{:T(128)}, f32[4,128,128]{2,1,0:T(8,128)S(1)}, f32[]{:T(128)}, s32[]{:T(128)}, bf16[16,4,128,128]{3,2,1,0:T(8,128)(2,1)}, /*index=5*/bf16[16]{...) while((s32[]{:T(128)}, f32[4,128,128]{2,1,0:T(8,128)S(1)}, ...), condition=%wide.region_5.7_spmd.clone, body=%wide.region_4.6_spmd.clone.sunk | while | flops 101056520 | bytes 1576144 | solution.py:34
  346.4 1.4 dynamic_slice.315
  352.8 1.3 dynamic_slice.315
  359.3 1.3 dynamic_slice.315
  365.7 1.3 dynamic_slice.315
  372.1 1.3 dynamic_slice.315
  378.6 1.3 dynamic_slice.315
  385.0 1.3 dynamic_slice.315
  391.5 1.3 dynamic_slice.315
  397.9 1.3 dynamic_slice.315
  404.3 1.3 dynamic_slice.315
  410.8 1.3 dynamic_slice.315
  417.2 1.3 dynamic_slice.315
  423.6 1.3 dynamic_slice.315
  430.1 1.3 dynamic_slice.315
  442.9 1.3 dynamic_slice.315
  450.1 56.9 %while.87 = (s32[]{:T(128)}, f32[4,128,128]{2,1,0:T(8,128)S(1)}, s32[]{:T(128)}, f32[2,4,64,128]{3,2,0,1:T(8,128)}, f32[2,4,64]{2,1,0:T(4,128)}, /*index=5*/s32[...) while((s32[]{:T(128)}, f32[4,128,128]{2,1,0:T(8,128)S(1)}, ...), condition=%wide.region_9.12_spmd, body=%wide.region_7.11_spmd.sunk | while | flops 277521280 | bytes 6467220 | solution.py:127
  452.7 19.7 %custom-call.19 = f32[4,1,64,64]{2,3,1,0:T(8,128)S(1)} custom-call(f32[4,1,64,64]{3,2,1,0:T(8,128)S(1)} %fusion.272), custom_call_target="InvertDiagBlocksLowerTriangular" | custom-call | tf_op jit(solution)/shard_map/while/body/eval_jaxpr/jit(_solve_triangular)/vmap()/triangular_solve | solution.py:67
  481.2 19.7 %custom-call.19 = f32[4,1,64,64]{2,3,1,0:T(8,128)S(1)} custom-call(f32[4,1,64,64]{3,2,1,0:T(8,128)S(1)} %fusion.272), custom_call_target="InvertDiagBlocksLowerTriangular" | custom-call | tf_op jit(solution)/shard_map/while/body/eval_jaxpr/jit(_solve_triangular)/vmap()/triangular_solve | solution.py:67
  512.5 13.0 %all-reduce.10.cloned.1.call-done = bf16[128,2048]{1,0:T(8,128)(2,1)} async-done(((bf16[128,2048]{1,0:T(8,128)(2,1)}), bf16[128,2048]{1,0:T(8,128)(2,1)}) %all-reduce.10.cloned.1.call-update) | async-done | bytes 524304 | tf_op jit(solution)/shard_map/psum | solution.py:294
  525.5 1.5 convert_add_fusion
  526.9 193.4 %all-gather.11.cloned.1.call-done = bf16[2048,4096]{1,0:T(8,128)(2,1)} async-done(((bf16[128,4096]{1,0:T(8,128)(2,1)}), bf16[2048,4096]{1,0:T(8,128)(2,1)}) %all-gather.11.cloned.1.call-update) | async-done | bytes 16777232 | tf_op jit(solution)/shard_map/all_gather | solution.py:304
  720.3 250.0 %all-gather.13.cloned.1.call-done = bf16[4096,2048]{1,0:T(8,128)(2,1)} async-done(((bf16[4096,128]{1,0:T(8,128)(2,1)}), bf16[4096,2048]{1,0:T(8,128)(2,1)}) %all-gather.13.cloned.1.call-update) | async-done | bytes 16777232 | tf_op jit(solution)/shard_map/all_gather | solution.py:310
  970.4 16.4 %convolution_convert_fusion = bf16[128,2048]{1,0:T(8,128)(2,1)} fusion(bf16[4096,2048]{1,0:T(8,128)(2,1)} %all-gather.13.cloned.1.call-done, bf16[2048,4096]{1,0:T(8,128)(2,1)} %all-gather.11.cloned.1.call-done, f32[2048]{0:T(1024)S(1)} %copy-done.16, f32[128]{0:T(128)S(1)} %add_rsqrt_fusion.3, bf16[128,2048]{1,0:T(8,128)(2,1)} %all-reduce.10.cloned.1.call-done, ...), kind=kOutput, calls=%fused_computation.245 | convolution fusion | flops 4298375168 | bytes 35136000 | tf_op jit(solution)/shard_map/dot_general | solution.py:308
  986.8 6.3 reduce-scatter.2.cloned.1.call-done
  993.0 1.7 add_convert_fusion
  (411 shorter events, 173.3 us)
Async XLA Ops:
  6.5 503.0 %copy-start = (bf16[512,2048]{1,0:T(8,128)(2,1)S(1)}, bf16[512,2048]{1,0:T(8,128)(2,1)}, u32[]{:S(2)}) copy-start(bf16[512,2048]{1,0:T(8,128)(2,1)} %param.40) | copy-start | bytes 6291460
  6.5 4.0 copy-start.11
  6.5 5.4 copy-start.21
  6.5 5.4 copy-start.18
  6.5 5.4 copy-start.17
  6.5 6.8 copy-start.19
  6.6 201.0 %all-gather.19.cloned.1.call-start = ((), (), s32[]{:S(2)}) async-start(), calls=%async_computation.7 | async-start | bytes 2228224 | tf_op jit(solution)/shard_map/all_gather | solution.py:16
  7.5 7.9 copy-start.23
  10.0 5.4 copy-start.5
  10.7 4.7 copy-start.6
  76.4 4.5 copy-start.20
  76.4 6.1 copy-start.14
  76.4 6.8 copy-start.15
  77.3 130.3 %all-gather.21.cloned.1.call-start = ((), (), s32[]{:S(2)}) async-start(), calls=%async_computation.8 | async-start | bytes 2228224 | tf_op jit(solution)/shard_map/all_gather | solution.py:16
  78.0 268.3 %all-gather.15.cloned.1.call-start = ((), (), s32[]{:S(2)}) async-start(), calls=%async_computation.5 | async-start | bytes 2228224 | tf_op jit(solution)/shard_map/all_gather | solution.py:16
  80.9 3.8 copy-start.3
  144.1 10.4 %copy-start.22 = (u32[32]{0:T(128)S(1)}, u32[32]{0:T(128)}, u32[]{:S(2)}) copy-start(u32[32]{0:T(128)} %constant.207) | copy-start | bytes 388
  144.9 201.4 %all-gather.17.cloned.1.call-start = ((), (), s32[]{:S(2)}) async-start(), calls=%async_computation.6 | async-start | bytes 2228224 | tf_op jit(solution)/shard_map/all_gather | solution.py:16
  145.5 380.0 %all-reduce.10.cloned.1.call-start = ((), (), s32[]{:S(2)}) async-start(), calls=%async_computation.1 | async-start | bytes 1048576 | tf_op jit(solution)/shard_map/psum | solution.py:294
  305.5 4.9 copy-start.2
  305.5 4.9 copy-start.9
  305.5 5.3 copy-start.12
  310.8 1.1 copy-start.10
  335.5 4.9 copy-start.2
  335.6 4.9 copy-start.9
  335.6 5.3 copy-start.12
  340.9 1.1 copy-start.10
  346.3 103.8 %copy-start.1 = (f32[4,128,128]{2,1,0:T(8,128)S(1)}, f32[4,128,128]{2,1,0:T(8,128)}, u32[]{:S(2)}) copy-start(f32[4,128,128]{2,1,0:T(8,128)} %copy.95) | copy-start | bytes 786436
  346.3 103.8 %copy-start.4 = (f32[4,128,128]{2,1,0:T(8,128)S(1)}, f32[4,128,128]{2,1,0:T(8,128)}, u32[]{:S(2)}) copy-start(f32[4,128,128]{2,1,0:T(8,128)} %copy-done.3) | copy-start | bytes 786436
  472.4 3.1 copy-start.7
  472.4 3.5 copy-start.13
  475.9 1.3 copy-start.8
  500.8 3.1 copy-start.7
  500.9 3.5 copy-start.13
  504.3 1.3 copy-start.8
  510.8 459.5 %copy-start.16 = (f32[2048]{0:T(1024)S(1)}, f32[2048]{0:T(1024)}, u32[]{:S(2)}) copy-start(f32[2048]{0:T(1024)} %param.41) | copy-start | bytes 24580
  510.9 209.5 %all-gather.11.cloned.1.call-start = ((), (), s32[]{:S(2)}) async-start(), calls=%async_computation.2 | async-start | bytes 17825792 | tf_op jit(solution)/shard_map/all_gather | solution.py:304
  511.4 458.9 %all-gather.13.cloned.1.call-start = ((), (), s32[]{:S(2)}) async-start(), calls=%async_computation.3 | async-start | bytes 17825792 | tf_op jit(solution)/shard_map/all_gather | solution.py:310
  512.2 480.8 %reduce-scatter.2.cloned.1.call-start = ((), (), s32[]{:S(2)}) async-start(), calls=%async_computation.4 | async-start | bytes 786432 | tf_op jit(solution)/shard_map/reduce_scatter | solution.py:314
Sparse Core Ops, SparseCore 0:
  77.4 64.2 all-gather.18
  144.4 59.3 all-gather.20
  206.6 59.2 all-gather.14
  268.4 60.8 all-gather.16
  511.0 14.4 all-reduce.9
  528.1 192.1 all-gather.10
  723.0 247.2 all-gather.12
  986.9 6.0 reduce-scatter.1
where the time goes:
time: 1010 us; the launch traced here: 1000 us
  waiting for transfers between devices  465 us (46%)
  other arithmetic  192 us (19%)
  local copies, waits for them, and re-layouts  114 us (11%)
  loops' own time  88.3 us (9%)
  matrix products  82.7 us (8%)
  blocking collectives  45 us (4%)
  between operations  13.9 us (1%)
    all_gather x1, waiting for transfers between devices, shards(): lax.all_gather(shrink_projection_weights, 'sp', axis=1, tiled=True)  250 us
    all_gather x1, waiting for transfers between devices, shards(): lax.all_gather(widen_projection_weights, 'sp', axis=0, tiled=True)  193 us
    another operation x16, other arithmetic, block_pass(): jax.scipy.linalg.solve_triangular(system, right_side, lower=True, unit_di...  160 us
    another operation x2, loops' own time, entering(): return lax.fori_loop(0, length, hop, start)  77.3 us
    dynamic_slice x64, local copies, waits for them, and re-layouts, hop(): part[at].astype(own.dtype)  59.4 us
    unnamed x1, blocking collectives  45 us
    dot_general x32, matrix products, compose(): jnp.einsum('hij,hjk->hik', late_map, early_shift, precision=HIGH) * joined  40.6 us
  transfers between devices with their start and end apart: 8, of which 4 were waited for; matrix products, arithmetic and copies ran while one was open for 18% of the time, Pallas kernels for 0%

commit v1 on v0

v1 whole, which is shorter than its diff:
```python
import functools

import jax
import jax.numpy as jnp
from jax import lax
from jax.experimental import pallas as pl
from jax.experimental.pallas import tpu as pltpu
from jax.sharding import PartitionSpec as P

EPSILON = 1e-06
F32 = jnp.float32
BF16 = jnp.bfloat16
MESH = pl.DeviceIdType.MESH


def mm(a, b, dims=((1,), (0,))):
    return lax.dot_general(
        a.astype(BF16), b.astype(BF16), (dims, ((), ())), preferred_element_type=F32
    )


def exact_mm(a, b, dims=((1,), (0,))):
    return lax.dot_general(
        a, b, (dims, ((), ())), precision=lax.Precision.HIGHEST, preferred_element_type=F32
    )


def mixer_kernel(
    n_sp,
    group,
    width,
    q_ref,
    k_ref,
    v_ref,
    beta_ref,
    g_ref,
    gt_ref,
    doc_col_ref,
    doc_row_ref,
    join_ref,
    w1_ref,
    w2_ref,
    attn,
    reads,
    maps,
    w1g_ref,
    w2g_ref,
    w_send,
    w_recv,
    own_sem,
):
    me = lax.axis_index("sp")
    rows = q_ref.shape[0]
    heads = q_ref.shape[1] // width
    part = w1_ref.shape[1] // group
    depth = w1_ref.shape[0]

    barrier = pltpu.get_barrier_semaphore()

    def greet(d, carry):
        pl.semaphore_signal(
            barrier, inc=1, device_id={"sp": lax.rem(me + d, n_sp)}, device_id_type=MESH
        )
        return carry

    lax.fori_loop(1, n_sp, greet, 0)
    pl.semaphore_wait(barrier, n_sp - 1)

    def weight_copies(d):
        to = lax.rem(me + d, n_sp)
        at = pl.multiple_of(lax.rem(to, group) * part, part)
        wide = pltpu.make_async_remote_copy(
            src_ref=w1_ref.at[:, pl.ds(at, part)],
            dst_ref=w1g_ref.at[pl.ds(pl.multiple_of(me * depth, depth), depth), :],
            send_sem=w_send.at[0, d],
            recv_sem=w_recv.at[0, d],
            device_id={"sp": to},
            device_id_type=MESH,
        )
        shrink = pltpu.make_async_remote_copy(
            src_ref=w2_ref.at[pl.ds(at, part), :],
            dst_ref=w2g_ref.at[me],
            send_sem=w_send.at[1, d],
            recv_sem=w_recv.at[1, d],
            device_id={"sp": to},
            device_id_type=MESH,
        )
        return wide, shrink

    def send_weights(d, carry):
        for copy in weight_copies(d):
            copy.start()
        return carry

    here = pl.multiple_of(lax.rem(me, group) * part, part)
    own_wide = pltpu.make_async_copy(
        w1_ref.at[:, pl.ds(here, part)],
        w1g_ref.at[pl.ds(pl.multiple_of(me * depth, depth), depth), :],
        own_sem.at[0],
    )
    own_shrink = pltpu.make_async_copy(
        w2_ref.at[pl.ds(here, part), :], w2g_ref.at[me], own_sem.at[1]
    )
    lax.fori_loop(1, n_sp, send_weights, 0)
    own_wide.start()
    own_shrink.start()

    row_ids = lax.broadcasted_iota(jnp.int32, (rows, rows), 0)
    col_ids = lax.broadcasted_iota(jnp.int32, (rows, rows), 1)
    doc_col = doc_col_ref[...]
    doc_row = doc_row_ref[...]
    shared = doc_col == doc_row
    eye = (row_ids == col_ids).astype(F32)
    lower = (row_ids >= col_ids).astype(F32)
    upper = (row_ids <= col_ids).astype(F32)
    g = g_ref[...]
    gt = gt_ref[...]
    run_cols = (exact_mm(lower, g), exact_mm(upper, g))
    run_rows = (exact_mm(gt, upper), exact_mm(gt, lower))
    first = doc_col[0:1, :]
    last = doc_col[rows - 1 : rows, :]
    from_first = (doc_col == first).astype(F32)
    from_last = (doc_col == last).astype(F32)
    whole = (first == last).astype(F32)
    levels = []
    size = 1
    while size < rows:
        levels.append(
            (row_ids // (2 * size) == col_ids // (2 * size)) & (row_ids // size != col_ids // size)
        )
        size *= 2

    for h in range(heads):
        cols = slice(h * width, (h + 1) * width)
        q = q_ref[:, cols].astype(F32)
        k = k_ref[:, cols].astype(F32)
        v = v_ref[:, cols].astype(F32)
        q = q * lax.rsqrt(jnp.sum(q * q, axis=1, keepdims=True) + EPSILON) * width ** (-0.5)
        k = k * lax.rsqrt(jnp.sum(k * k, axis=1, keepdims=True) + EPSILON)
        keys = mm(k, k, ((1,), (1,)))
        probes = mm(q, k, ((1,), (1,)))
        total = None
        for w in range(2):
            u = w * heads + h
            run = run_cols[w][:, u : u + 1]
            gap = run - run_rows[w][u : u + 1, :]
            within = ((row_ids >= col_ids) if w == 0 else (row_ids <= col_ids)) & shared
            spread = jnp.where(within, jnp.exp(jnp.where(within, gap, 0.0)), 0.0)
            beta = beta_ref[:, u : u + 1]
            system = jnp.where(row_ids == col_ids, 0.0, keys * spread * beta)
            inverse = eye - jnp.where(levels[0], system, 0.0)
            for level in levels[1:]:
                inverse = inverse - mm(inverse, mm(jnp.where(level, system, 0.0), inverse))
            link = from_first if w == 0 else from_last
            ending = from_last if w == 0 else from_first
            fade = jnp.exp(run) * link
            right = jnp.concatenate([v * beta, k * (beta * fade)], axis=1)
            solved = mm(inverse, right)
            end = run[rows - 1 : rows, :] if w == 0 else run[0:1, :]
            faded = k * (jnp.exp(end - run) * ending)
            moved = mm(solved, faded, ((0,), (0,)))
            kept = jnp.exp(end) * whole
            join = join_ref[w : w + 1, :]
            maps[u, :width, :] = ((eye * kept - moved[width:, :]) * join).astype(BF16)
            maps[u, width:, :] = moved[:width, :].astype(BF16)
            scored = mm(probes * spread, solved)
            reads[u] = ((q * fade - scored[:, width:]) * join).astype(BF16)
            total = scored[:, :width] if w == 0 else total + scored[:, :width]
        attn[h] = total

    def weights_done(d, carry):
        for copy in weight_copies(d):
            copy.wait()
        return carry

    lax.fori_loop(1, n_sp, weights_done, 0)
    own_wide.wait()
    own_shrink.wait()


def finish_kernel(n_sp, attn, reads, gathered, gain_ref, mixed_ref, held):
    me = lax.axis_index("sp")
    units, _, width = reads.shape
    heads = units // 2

    held[...] = jnp.zeros_like(held)

    def hop_of(backward):
        def hop(n, carry):
            s = n_sp - 1 - n if backward else n
            for u in range(backward * heads, backward * heads + heads):
                held[u] = mm(held[u], gathered[s, u, :width, :]) + gathered[
                    s, u, width:, :
                ].astype(F32)
            return carry

        return hop

    lax.fori_loop(0, me, hop_of(0), 0)
    lax.fori_loop(0, n_sp - 1 - me, hop_of(1), 0)
    for h in range(heads):
        total = attn[h]
        for u in (h, heads + h):
            total = total + mm(reads[u], held[u], ((1,), (1,)))
        scaled = (
            total
            * lax.rsqrt(jnp.mean(total * total, axis=1, keepdims=True) + EPSILON)
            * gain_ref[...]
        )
        mixed_ref[:, h * width : (h + 1) * width] = scaled.astype(BF16)


def dense_kernel(
    n_tp,
    group,
    tile,
    x_ref,
    res_ref,
    w1_ref,
    w2_ref,
    out_ref,
    held,
    total,
    terms,
    landed,
    x_send,
    x_recv,
    p_send,
    p_recv,
):
    me = lax.axis_index("sp")
    core = lax.axis_index("tp")
    base = me // group * group
    place = me - base
    rows = x_ref.shape[0]
    part = w1_ref.shape[1]
    cols = out_ref.shape[1]

    barrier = pltpu.get_barrier_semaphore()
    for d in range(group):
        for e in range(n_tp):
            if d or e:
                pl.semaphore_signal(
                    barrier,
                    inc=1,
                    device_id={
                        "sp": base + lax.rem(place + d, group),
                        "tp": lax.rem(core + e, n_tp),
                    },
                    device_id_type=MESH,
                )
    pl.semaphore_wait(barrier, group * n_tp - 1)

    def x_copy(d):
        return pltpu.make_async_remote_copy(
            src_ref=x_ref,
            dst_ref=held.at[d],
            send_sem=x_send.at[d],
            recv_sem=x_recv.at[d],
            device_id={"sp": base + lax.rem(place + d, group)},
            device_id_type=MESH,
        )

    def p_copy(d, e):
        to = lax.rem(core + e, n_tp)
        return pltpu.make_async_remote_copy(
            src_ref=terms.at[d, to],
            dst_ref=landed.at[d, e],
            send_sem=p_send.at[d * n_tp + e],
            recv_sem=p_recv.at[d * n_tp + e],
            device_id={"sp": base + lax.rem(place - d + group, group), "tp": to},
            device_id_type=MESH,
        )

    for d in range(1, group):
        x_copy(d).start()

    held[0] = x_ref[...]
    for d in range(group):
        if d:
            x_copy(d).wait_recv()

        def step(i, carry):
            at = pl.multiple_of(i * tile, tile)
            raised = jnp.dot(
                held[d], w1_ref[:, pl.ds(at, tile)], preferred_element_type=F32
            )
            active = jnp.square(jnp.maximum(raised, 0.0)).astype(BF16)
            total[...] += jnp.dot(active, w2_ref[pl.ds(at, tile), :], preferred_element_type=F32)
            return carry

        total[...] = jnp.zeros_like(total)
        lax.fori_loop(0, part // tile, step, 0)
        for t in range(n_tp):
            terms[d, t] = total[:, t * cols : (t + 1) * cols].astype(BF16)
        for e in range(n_tp):
            if d or e:
                p_copy(d, e).start()

    summed = res_ref[...] + terms[0, core].astype(F32)
    for d in range(group):
        for e in range(n_tp):
            if d or e:
                p_copy(d, e).wait_recv()
                summed = summed + landed[d, e].astype(F32)
    out_ref[...] = summed.astype(out_ref.dtype)
    for d in range(1, group):
        x_copy(d).wait_send()
    for d in range(group):
        for e in range(n_tp):
            if d or e:
                p_copy(d, e).wait_send()


def shards(
    skip_path_inputs,
    probe_vectors,
    lookup_vectors,
    payload_vectors,
    learning_strength_preacts,
    forget_preacts,
    forgetting_speed_exponent,
    extra_forgetting_spikes,
    sample_membership,
    channel_group_scaling,
    blend_exit_weights,
    dense_block_scaling,
    widen_projection_weights,
    shrink_projection_weights,
):
    n_sp, n_tp = lax.axis_size("sp"), lax.axis_size("tp")
    me = lax.axis_index("sp")
    rows = probe_vectors.shape[0]
    width = channel_group_scaling.shape[0]
    heads = probe_vectors.shape[1] // width
    units = 2 * heads
    model_width = skip_path_inputs.shape[1]
    depth, hidden = widen_projection_weights.shape
    out_cols = shrink_projection_weights.shape[1]
    group = 4
    part = hidden // group

    beta = jax.nn.sigmoid(learning_strength_preacts)
    decay = (
        -jnp.exp(forgetting_speed_exponent)[:, None, :] * jax.nn.softplus(forget_preacts)
        + extra_forgetting_spikes
    )
    side = lambda a: jnp.transpose(a, (1, 0, 2)).reshape(rows, units)
    beta, decay = side(beta), side(decay)
    earlier = lax.ppermute(sample_membership[-1:], "sp", [(i, i + 1) for i in range(n_sp - 1)])
    later = lax.ppermute(sample_membership[:1], "sp", [(i + 1, i) for i in range(n_sp - 1)])
    joined = jnp.stack(
        [
            (earlier == sample_membership[:1]) & (me > 0),
            (later == sample_membership[-1:]) & (me < n_sp - 1),
        ]
    ).astype(F32)
    joined = jnp.broadcast_to(joined, (2, width))

    vmem = pl.BlockSpec(memory_space=pltpu.VMEM)
    anywhere = pl.BlockSpec(memory_space=pl.ANY)
    dma = pltpu.SemaphoreType.DMA
    attn, reads, maps, wide, shrink = pl.pallas_call(
        functools.partial(mixer_kernel, n_sp, group, width),
        out_shape=(
            jax.ShapeDtypeStruct((heads, rows, width), F32),
            jax.ShapeDtypeStruct((units, rows, width), BF16),
            jax.ShapeDtypeStruct((units, 2 * width, width), BF16),
            jax.ShapeDtypeStruct((depth * n_sp, part), BF16),
            jax.ShapeDtypeStruct((n_sp, part, out_cols), BF16),
        ),
        in_specs=[vmem] * 11,
        out_specs=(vmem, vmem, vmem, anywhere, anywhere),
        scratch_shapes=[
            dma((2, n_sp)),
            dma((2, n_sp)),
            dma((2,)),
        ],
        compiler_params=pltpu.CompilerParams(
            collective_id=0, has_side_effects=True, vmem_limit_bytes=40 * 1024 * 1024
        ),
        name="mixer",
    )(
        probe_vectors,
        lookup_vectors,
        payload_vectors,
        beta,
        decay,
        decay.T,
        sample_membership[:, None],
        sample_membership[None, :],
        joined,
        widen_projection_weights,
        shrink_projection_weights,
    )
    mixed = pl.pallas_call(
        functools.partial(finish_kernel, n_sp),
        out_shape=jax.ShapeDtypeStruct((rows, heads * width), BF16),
        in_specs=[vmem] * 4,
        out_specs=vmem,
        scratch_shapes=[pltpu.VMEM((units, width, width), F32)],
        compiler_params=pltpu.CompilerParams(vmem_limit_bytes=40 * 1024 * 1024),
        name="finish",
    )(attn, reads, lax.all_gather(maps, "sp"), channel_group_scaling[None, :])
    shrink = jnp.transpose(shrink, (1, 0, 2)).reshape(part, n_sp * out_cols)

    head_terms = jnp.dot(mixed, blend_exit_weights, preferred_element_type=F32).astype(BF16)
    col_count = model_width // n_tp
    col_start = lax.axis_index("tp") * col_count
    residual = skip_path_inputs.astype(F32) + lax.psum(head_terms, "tp").astype(F32)
    normed = (
        residual
        * lax.rsqrt(jnp.mean(residual * residual, axis=1, keepdims=True) + EPSILON)
        * dense_block_scaling
    ).astype(BF16)
    own_residual = lax.dynamic_slice_in_dim(residual, col_start, col_count, 1)
    return pl.pallas_call(
        functools.partial(dense_kernel, n_tp, group, min(part, 256)),
        out_shape=jax.ShapeDtypeStruct((rows, col_count), BF16),
        in_specs=[vmem] * 4,
        out_specs=vmem,
        scratch_shapes=[
            pltpu.VMEM((group, rows, model_width), BF16),
            pltpu.VMEM((rows, model_width), F32),
            pltpu.VMEM((group, n_tp, rows, col_count), BF16),
            pltpu.VMEM((group, n_tp, rows, col_count), BF16),
            dma((group,)),
            dma((group,)),
            dma((group * n_tp,)),
            dma((group * n_tp,)),
        ],
        compiler_params=pltpu.CompilerParams(
            collective_id=1, has_side_effects=True, vmem_limit_bytes=48 * 1024 * 1024
        ),
        name="dense",
    )(normed, own_residual, wide, shrink)


def solution(mesh):
    placed = (
        P("sp", None),
        P("sp", "tp"),
        P("sp", "tp"),
        P("sp", "tp"),
        P(None, "sp", "tp"),
        P(None, "sp", "tp"),
        P(None, "tp"),
        P(None, "sp", "tp"),
        P("sp"),
        P(),
        P("tp", None),
        P(),
        P("sp", "tp"),
        P("tp", "sp"),
    )
    return jax.shard_map(
        shards, mesh=mesh, in_specs=placed, out_specs=P("sp", "tp"), check_vma=False
    )
```

time: 1010 us -> 461 us (0.46)
  waiting for transfers between devices: 465 us -> 175 us
  Pallas kernels: 0 us -> 234 us
  other arithmetic: 192 us -> 4.95 us
  local copies, waits for them, and re-layouts: 114 us -> 21.8 us
  loops' own time: 88.3 us -> 0 us
  matrix products: 82.7 us -> 1.25 us
  blocking collectives: 45 us -> 0 us
    all_gather x6 -> x1, waiting for transfers between devices: 443 us -> 163 us  [shards(): lax.all_gather(maps, 'sp')]
    pallas_call x0 -> x3, Pallas kernels: none -> 234 us  [the longest x1 174 us: shards(): pl.pallas_call(functools.partial(mixer_kernel, n_sp, group, width), out_s...]
    another operation x28 -> x0, other arithmetic: 164 us -> none  [the longest x16 160 us: block_pass(): jax.scipy.linalg.solve_triangular(system, right_side, lower=True, unit_di...]
    another operation x6 -> x0, loops' own time: 88.3 us -> none  [the longest x2 77.3 us: entering(): return lax.fori_loop(0, length, hop, start)]
    dot_general x70 -> x1, matrix products: 78.9 us -> 1.25 us  [shards(): jnp.dot(mixed, blend_exit_weights, preferred_element_type=F32).astype(BF16)]
    dynamic_slice x64 -> x1, local copies, waits for them, and re-layouts: 59.4 us -> 0.05 us  [shards(): own_residual = lax.dynamic_slice_in_dim(residual, col_start, col_count, 1)]
    unnamed x1 -> x0, blocking collectives: 45 us -> none
    slice x31 -> x1, local copies, waits for them, and re-layouts: 16.6 us -> 1.41 us  [shards(): sample_membership[-1:]]
  transfers between devices with their start and end apart: 8 -> 4, of which waited for: 4 -> 2; matrix products, arithmetic and copies ran while one was open for 18% -> 2% of each run, Pallas kernels for 0% -> 0%
where the time goes in v1:
time: 461 us; the launch traced here: 460 us
  Pallas kernels  234 us (51%)
  waiting for transfers between devices  175 us (38%)
  local copies, waits for them, and re-layouts  21.8 us (5%)
  between operations  16.1 us (3%)
  starting transfers between devices  6.73 us (1%)
  other arithmetic  4.95 us (1%)
    pallas_call x1, Pallas kernels, shards(): pl.pallas_call(functools.partial(mixer_kernel, n_sp, group, width), out_s...  174 us
    all_gather x1, waiting for transfers between devices, shards(): lax.all_gather(maps, 'sp')  163 us
    pallas_call x1, Pallas kernels, shards(): pl.pallas_call(functools.partial(dense_kernel, n_tp, group, min(part, 256...  56.6 us
    unnamed x29, local copies, waits for them, and re-layouts  14.5 us
    psum x1, waiting for transfers between devices, shards(): lax.psum(head_terms, 'tp').astype(F32)  12.1 us
  transfers between devices with their start and end apart: 4, of which 2 were waited for; matrix products, arithmetic and copies ran while one was open for 2% of the time, Pallas kernels for 0%

profile of v1, /device:TPU:0, one launch (start us, length us, event | category | flops | bytes accessed | tf_op | source)
XLA Modules:
  0.0 460.2 jit_solution(1382005139419556782)
XLA Ops:
  6.5 0.0 copy-start
  6.5 0.0 all-gather.3.cloned.1.call-start
  6.5 1.4 fusion.2
  8.0 5.4 %collective-permute-start = (s32[1]{0:T(128)}, s32[1]{0:T(128)}, u32[]{:S(2)}, u32[]{:S(2)}) collective-permute-start(s32[1]{0:T(128)} %get-tuple-element.17), channel_id=1, source_target_pairs={{0,2},{2,4},{4,6},{6,8},{8,10},{10,12},{12,14},{14,16},{16,18},{18... | collective-permute-start | bytes 20 | tf_op jit(solution)/shard_map/ppermute | solution.py:350
  13.4 1.3 collective-permute-start.1
  14.7 0.7 exponential_negate_fusion
  15.3 0.7 add_divide_fusion
  16.0 0.1 copy.23.beta_ref
  16.1 0.8 fusion.1
  16.9 0.1 copy.24.g_ref
  17.0 0.8 copy.25.doc_col_ref
  17.8 0.0 collective-permute-done
  19.1 0.0 collective-permute-done.1
  20.3 0.1 add_convert_fusion
  20.4 0.1 broadcast_in_dim.19.join_ref
  20.5 0.0 copy-start.5
  20.5 1.2 copy-done.5
  21.7 0.0 copy-start.6
  21.7 1.2 copy-done.6
  22.9 0.0 copy-start.7
  22.9 0.9 copy-done.7
  23.9 0.9 copy-done.8
  24.8 0.9 copy-done.9
  25.7 0.7 copy-done.10
  26.3 174.2 %mixer.1 = (f32[4,128,128]{2,1,0:T(8,128)S(1)}, bf16[8,128,128]{2,1,0:T(8,128)(2,1)S(1)}, bf16[8,256,128]{2,1,0:T(8,128)(2,1)}, bf16[2048,1024]{1,0:T(8,128)(2,1)S(1)}, bf16[16,1024,128]{2,1,0:T(8,128)(2,1)S(1)}) custom-call(bf16[128,512]{1,0:T(8,128)(2,1)S(1)} %copy-done.7, bf16[128,512]{1,0:T(8,128)(2,1)S(1)} %copy-done.8, bf16[128,512]{1,0:T(8,128)(2,1)S(1)} %copy-done.9, ...), custom_call_target="tpu_custom_call" | custom-call | tf_op jit(solution)/shard_map/mixer/pallas_call | solution.py:363
  200.6 0.0 copy-start.2
  200.6 2.0 copy-done.2
  202.6 1.9 copy-done.4
  204.5 0.0 all-gather.3.cloned.1.call-update
  204.5 0.0 all-reduce.2.cloned.1.call-start
  204.5 163.3 %all-gather.3.cloned.1.call-done = bf16[128,256,128]{2,1,0:T(8,128)(2,1)} async-done(((bf16[8,256,128]{2,1,0:T(8,128)(2,1)}), bf16[128,256,128]{2,1,0:T(8,128)(2,1)}) %all-gather.3.cloned.1.call-update) | async-done | bytes 8388624 | tf_op jit(solution)/shard_map/all_gather | solution.py:404
  367.9 3.4 copy-done.1
  371.2 0.7 copy-done.11
  371.9 3.1 finish.1
  375.0 0.0 copy-done
  375.0 1.3 convolution_convert_fusion
  376.3 0.0 all-reduce.2.cloned.1.call-update
  376.3 0.0 copy-start.12
  376.3 0.0 copy-start.13
  376.3 4.8 %copy_bitcast_fusion.w2_ref = bf16[1024,2048]{1,0:T(8,128)(2,1)} fusion(bf16[16,1024,128]{2,1,0:T(8,128)(2,1)} %copy-done.4), kind=kLoop, calls=%fused_computation | loop fusion | bytes 8388608 | tf_op jit(solution)/shard_map/reshape | solution.py:405
  381.1 12.1 %all-reduce.2.cloned.1.call-done = bf16[128,2048]{1,0:T(8,128)(2,1)} async-done(((bf16[128,2048]{1,0:T(8,128)(2,1)}), bf16[128,2048]{1,0:T(8,128)(2,1)}) %all-reduce.2.cloned.1.call-update) | async-done | bytes 524304 | tf_op jit(solution)/shard_map/psum | solution.py:410
  393.2 0.0 copy-done.12
  393.2 1.4 convert_add_fusion
  394.7 0.0 copy-done.13
  394.7 1.3 multiply_convert_fusion.x_ref
  396.0 0.0 copy-done.3
  396.0 56.6 %dense.1 = bf16[128,1024]{1,0:T(8,128)(2,1)S(1)} custom-call(bf16[128,2048]{1,0:T(8,128)(2,1)S(1)} %multiply_convert_fusion.x_ref, f32[128,1024]{1,0:T(8,128)S(1)} %constant_dynamic-slice_fusion.res_ref, bf16[2048,1024]{1,0:T(8,128)(2,1)S(1)} %copy-done.3, bf16[1024,2048]{1,0:T(8,128)(2,1)} %copy_bitcast_fusion.w2_ref), custom_call_target="tpu_custom_call" | custom-call | tf_op jit(solution)/shard_map/dense/pallas_call | solution.py:417
  452.7 0.7 copy.31
  (9 shorter events, 0.1 us)
Async XLA Ops:
  6.5 368.5 %copy-start = (bf16[512,2048]{1,0:T(8,128)(2,1)S(1)}, bf16[512,2048]{1,0:T(8,128)(2,1)}, u32[]{:S(2)}) copy-start(bf16[512,2048]{1,0:T(8,128)(2,1)} %param.24) | copy-start | bytes 6291460
  6.5 361.3 %all-gather.3.cloned.1.call-start = ((), (), s32[]{:S(2)}) async-start(), calls=%async_computation.1 | async-start | bytes 8912896 | tf_op jit(solution)/shard_map/all_gather | solution.py:404
  8.0 9.8 %collective-permute-start = (s32[1]{0:T(128)}, s32[1]{0:T(128)}, u32[]{:S(2)}, u32[]{:S(2)}) collective-permute-start(s32[1]{0:T(128)} %get-tuple-element.17), channel_id=1, source_target_pairs={{0,2},{2,4},{4,6},{6,8},{8,10},{10,12},{12,14},{14,16},{16,18},{18... | collective-permute-start | bytes 20 | tf_op jit(solution)/shard_map/ppermute | solution.py:350
  13.4 5.8 %collective-permute-start.1 = (s32[1]{0:T(128)}, s32[1]{0:T(128)}, u32[]{:S(2)}, u32[]{:S(2)}) collective-permute-start(s32[1]{0:T(128)} %get-tuple-element.18), channel_id=1, source_target_pairs={{2,0},{4,2},{6,4},{8,6},{10,8},{12,10},{14,12},{16,14},{18,16},{20... | collective-permute-start | bytes 20 | tf_op jit(solution)/shard_map/ppermute | solution.py:351
  20.5 1.2 copy-start.5
  21.7 1.2 copy-start.6
  22.9 0.9 copy-start.7
  23.9 0.9 copy-start.8
  24.8 0.9 copy-start.9
  25.7 0.7 copy-start.10
  200.6 2.0 copy-start.2
  202.5 1.9 copy-start.4
  204.5 188.7 %all-reduce.2.cloned.1.call-start = ((), (), s32[]{:S(2)}) async-start(), calls=%async_computation | async-start | bytes 1048576 | tf_op jit(solution)/shard_map/psum | solution.py:410
  367.9 3.4 copy-start.1
  371.2 0.7 copy-start.11
  376.3 16.9 %copy-start.12 = (bf16[128,2048]{1,0:T(8,128)(2,1)S(1)}, bf16[128,2048]{1,0:T(8,128)(2,1)}, u32[]{:S(2)}) copy-start(bf16[128,2048]{1,0:T(8,128)(2,1)} %param.14) | copy-start | bytes 1572868
  376.3 18.4 %copy-start.13 = (f32[2048]{0:T(1024)S(1)}, f32[2048]{0:T(1024)}, u32[]{:S(2)}) copy-start(f32[2048]{0:T(1024)} %param.25) | copy-start | bytes 24580
  393.2 2.8 copy-start.3
Sparse Core Ops, SparseCore 0:
  204.6 163.2 all-gather.2
  376.4 16.7 all-reduce.1
